TPU v7x, 32 devices: a whole 2x2x4 slice. The times are simulated.
32 devices in a mesh: gr: 2 (over y), sp: 4 (over z), tp: 4 (over x, core).
Axes of the slice: x: 2, y: 2, z: 4, core: 2. Of those that a mesh axis runs over, the one named last changes fastest.
Arguments:
- tokens: bfloat16 [8, 8192, 2048], P(('gr', 'tp'), 'sp'), may hold values from -6 to 6
- kv_weight: bfloat16 [2048, 1024], replicated, may hold values from -0.125 to 0.125
- queries: bfloat16 [8, 1536], P(('gr', 'tp')), may hold values from -6 to 6
- score_offset: float32 [24], replicated, may hold values from -10.5 to -3.5
Outputs:
- cache: bfloat16 [8, 4, 8192, 256], P(('gr', 'tp'), 'sp')
- read: bfloat16 [8, 1536], P(('gr', 'tp'))
All inputs are finite; a program needn't handle non-finite values.
Results may differ from a plain program's by a relative error of at most 0.0085.
Values may be sent and summed in bfloat16 or wider, within the bound.
A program may use at most 64 MiB of HBM per device.

v0:
```python
import jax
import jax.numpy as jnp
from jax import lax
from jax.sharding import PartitionSpec as P

KVH = 8
HD = 64


def prefix(shard, axis, combine, identity):
    size, index = (lax.axis_size(axis), lax.axis_index(axis))
    everything = lax.all_gather(shard, axis)
    start = jnp.broadcast_to(jnp.asarray(identity, shard.dtype), shard.shape)

    def hop(k, before):
        at = size - 1 - k
        reached = at > index
        new = combine(before, everything[at])
        return jnp.where(reached, new, before)

    return lax.fori_loop(0, size, hop, start)


def add_terms(earlier, later):
    return earlier + later


def finish(contribution):
    return lax.psum(contribution, "sp").astype(jnp.bfloat16)


def local(tokens, kv_weight, queries, score_offset):
    seq_count, pos_rows, model_width = tokens.shape
    features = kv_weight.shape[1]
    slot_count = lax.axis_size("sp")
    blocks = slot_count // seq_count
    block_width = features // blocks
    half_blocks = blocks // 2
    heads = score_offset.shape[0]
    group_size = heads // KVH
    per_block = block_width // HD
    projected = jnp.einsum(
        "spd,dcw->scpw",
        tokens,
        kv_weight.reshape(model_width, blocks, block_width),
        preferred_element_type=jnp.float32,
    ).astype(jnp.bfloat16)
    received = lax.all_to_all(
        projected.reshape(slot_count, pos_rows, block_width),
        "sp",
        split_axis=0,
        concat_axis=1,
        tiled=True,
    )
    length = received.shape[1]
    cache = received.reshape(1, 1, length, block_width)
    key_part = projected[:, :half_blocks].reshape(seq_count, half_blocks, pos_rows, per_block, HD)
    value_part = (
        projected[:, half_blocks:]
        .reshape(seq_count, half_blocks, pos_rows, per_block, HD)
        .astype(jnp.float32)
    )
    query_heads = queries.reshape(seq_count, half_blocks, per_block, group_size, HD)
    offsets = score_offset.reshape(half_blocks, per_block, group_size)
    logits = jnp.einsum(
        "scvgd,scpvd->scvgp", query_heads, key_part, preferred_element_type=jnp.float32
    )
    logits = logits * HD ** (-0.5) + offsets[None, :, :, :, None]
    keep_log = jax.nn.log_sigmoid(-logits)
    between = lax.cumsum(keep_log, axis=4, reverse=True) - keep_log
    totals = jnp.sum(keep_log, axis=4)
    later_keep = prefix(totals, "sp", add_terms, jnp.zeros_like(totals))
    weights = jnp.exp(jax.nn.log_sigmoid(logits) + between + later_keep[..., None])
    weighted = jnp.einsum("scvgp,scpvd->scvgd", weights, value_part)
    contribution = weighted.reshape(seq_count, heads * HD)
    return (cache, finish(contribution))


def solution(mesh):
    placed = (P(("gr", "tp"), "sp", None), P(), P(("gr", "tp"), None), P())
    return jax.shard_map(
        local,
        mesh=mesh,
        in_specs=placed,
        out_specs=(P(("gr", "tp"), "sp", None, None), P(("gr", "tp"), None)),
        check_vma=False,
    )
```

profile of v0, /device:TPU:0, one launch (start us, length us, event | category | flops | bytes accessed | tf_op | source)
XLA Modules:
  0.0 152.8 jit_solution(13266032092984651782)
XLA Ops:
  0.6 6.4 %copy.34 = bf16[2048,1024]{0,1:T(8,128)(2,1)} copy(bf16[2048,1024]{1,0:T(8,128)(2,1)} %param.7) | data formatting | bytes 8388608 | tf_op jit(solution)/shard_map/reshape | solution.py:45
  7.1 13.9 %fusion.2 = bf16[4,256,2048]{2,1,0:T(8,128)(2,1)} fusion(bf16[2048,4,256]{0,2,1:T(8,128)(2,1)} %bitcast.41, bf16[1,2048,2048]{2,1,0:T(8,128)(2,1)} %param.6), kind=kOutput, calls=%fused_computation.3 | convolution fusion | flops 8592031744 | bytes 16777216 | tf_op jit(solution)/shard_map/spd,dcw->scpw/dot_general | solution.py:42
  21.0 6.5 %all-to-all-start = ((bf16[4,2048,256]{1,2,0:T(8,128)(2,1)}), bf16[4,2048,256]{1,2,0:T(8,128)(2,1)}, u32[]{:S(2)}, u32[]{:S(2)}) async-start(bf16[4,2048,256]{1,2,0:T(8,128)(2,1)} %bitcast.38), calls=%async_computation | async-start | bytes 8388608 | tf_op jit(solution)/shard_map/all_to_all | solution.py:48
  27.5 0.1 reshape.113
  27.6 0.1 add.81
  27.7 2.8 %fusion.28 = (bf16[1,2,2048,256]{2,3,1,0:T(8,128)(2,1)S(1)}, bf16[1,2,2048,256]{2,3,1,0:T(8,128)(2,1)S(1)}) fusion(bf16[1,4,2048,256]{2,3,1,0:T(8,128)(2,1)} %bitcast.39), kind=kLoop, calls=%fused_computation.29 | loop fusion | bytes 8388608 | tf_op jit(solution)/shard_map/slice | solution.py:57
  30.4 0.7 fusion.24
  31.1 0.1 reshape.123
  31.2 29.8 %reduce-window.6 = f32[1,2,4,3,16,128]{5,4,3,2,1,0:T(8,128)S(1)} reduce-window(f32[1,2,4,3,16,128]{5,4,3,2,1,0:T(8,128)S(1)} %reshape.123, f32[]{:T(128)} %constant.56.clone.1), window={size=1x1x1x1x1x128 pad=0_0x0_0x0_0x0_0x0_0x0_127}, to_apply=%region_0.1 | reduce-window | flops 6242304 | bytes 393220 | tf_op jit(solution)/shard_map/reduce-window
  61.0 0.1 reshape.124
  61.1 0.2 copy.37
  61.3 1.5 reduce-window.9
  62.8 0.1 slice_bitcast_fusion
  62.9 0.1 broadcast.20
  63.0 0.1 reshape.118
  63.1 63.1 %all-gather = f32[8,4,3]{2,1,0:T(4,128)S(1)} all-gather(f32[2,4,3]{2,1,0:T(4,128)S(1)} %neg.35), channel_id=2, replica_groups=mesh['gr'=2,'sp'=4,'tp'=4] {'sp'}, dimensions={0}, use_global_device_ids=true | all-gather | bytes 480 | tf_op jit(solution)/shard_map/all_gather | solution.py:12
  126.2 0.1 copy.32
  126.3 0.2 while.16
  126.5 0.1 copy.33
  126.6 0.9 fusion.11
  127.6 0.1 reshape.120
  127.7 18.9 %psum.7 = bf16[1,1536]{1,0:T(2,128)(2,1)} all-reduce(f32[1,1536]{1,0:T(1,128)S(1)} %reshape.120), channel_id=1, replica_groups=mesh['gr'=2,'sp'=4,'tp'=4] {'sp'}, use_global_device_ids=true, to_apply=%region_5.6 | all-reduce | flops 1536 | bytes 9216 | tf_op jit(solution)/shard_map/psum | solution.py:29
  146.6 0.0 all-to-all-done
  146.6 6.2 %copy.22 = bf16[4,2048,256]{2,1,0:T(8,128)(2,1)} copy(bf16[4,2048,256]{1,2,0:T(8,128)(2,1)} %all-to-all-done) | data formatting | bytes 8388608 | tf_op jit(solution)/shard_map/all_to_all | solution.py:48
  (12 shorter events, 0.1 us)
Async XLA Ops:
  21.0 6.5 %copy-start = (bf16[1,1536]{1,0:T(2,128)(2,1)S(1)}, bf16[1,1536]{1,0:T(2,128)(2,1)}, u32[]{:S(2)}) copy-start(bf16[1,1536]{1,0:T(2,128)(2,1)} %param.8) | copy-start | bytes 9220
  21.0 6.6 %copy-start.1 = (f32[24]{0:T(128)S(1)}, f32[24]{0:T(128)}, u32[]{:S(2)}) copy-start(f32[24]{0:T(128)} %param.9) | copy-start | bytes 292
  21.0 125.6 %all-to-all-start = ((bf16[4,2048,256]{1,2,0:T(8,128)(2,1)}), bf16[4,2048,256]{1,2,0:T(8,128)(2,1)}, u32[]{:S(2)}, u32[]{:S(2)}) async-start(bf16[4,2048,256]{1,2,0:T(8,128)(2,1)} %bitcast.38), calls=%async_computation | async-start | bytes 8388608 | tf_op jit(solution)/shard_map/all_to_all | solution.py:48
where the time goes:
time: 153 us
  blocking collectives  82 us (54%)
  other arithmetic  31.4 us (21%)
  local copies, waits for them, and re-layouts  16.6 us (11%)
  matrix products  15.5 us (10%)
  starting transfers between devices  6.47 us (4%)
    all_gather x1, blocking collectives, prefix(): everything = lax.all_gather(shard, axis)  63.1 us
    another operation x2, other arithmetic  31.3 us
    psum x1, blocking collectives, finish(): return lax.psum(contribution, 'sp').astype(jnp.bfloat16)  18.9 us
    dot_general x1, matrix products, local(): jnp.einsum('spd,dcw->scpw', tokens, kv_weight.reshape(model_width, blocks...  13.9 us
    all_to_all x1, starting transfers between devices, local(): lax.all_to_all(projected.reshape(slot_count, pos_rows, block_width), 'sp'...  6.47 us
    reshape x1, local copies, waits for them, and re-layouts, local(): kv_weight.reshape(model_width, blocks, block_width)  6.43 us
    all_to_all x1, local copies, waits for them, and re-layouts, local(): lax.all_to_all(projected.reshape(slot_count, pos_rows, block_width), 'sp'...  6.18 us
  transfers between devices with their start and end apart: 1, of which 0 were waited for; matrix products, arithmetic and copies ran while one was open for 24% of the time, Pallas kernels for 0%

commit v1 on v0

--- a/solution.py
+++ b/solution.py
@@ -26,7 +26,7 @@
 
 
 def finish(contribution):
-    return lax.psum(contribution, "sp").astype(jnp.bfloat16)
+    return jnp.sum(lax.all_gather(contribution, "sp"), axis=0).astype(jnp.bfloat16)
 
 
 def local(tokens, kv_weight, queries, score_offset):

time: 153 us -> 148 us (0.967)
  blocking collectives: 82 us -> 76.2 us
    psum x1 -> x0, blocking collectives: 18.9 us -> none  [finish(): return lax.psum(contribution, 'sp').astype(jnp.bfloat16)]
    all_gather x0 -> x1, blocking collectives: none -> 13.2 us  [finish(): lax.all_gather(contribution, 'sp')]
  transfers between devices with their start and end apart: 1 -> 1, of which waited for: 0 -> 0; matrix products, arithmetic and copies ran while one was open for 24% -> 25% of each run, Pallas kernels for 0% -> 0%
where the time goes in v1:
time: 148 us
  blocking collectives  76.2 us (51%)
  other arithmetic  31.4 us (21%)
  local copies, waits for them, and re-layouts  17.2 us (12%)
  matrix products  15.5 us (10%)
  starting transfers between devices  6.47 us (4%)
    all_gather x1, blocking collectives, prefix(): everything = lax.all_gather(shard, axis)  63.1 us
    another operation x2, other arithmetic  31.3 us
    dot_general x1, matrix products, local(): jnp.einsum('spd,dcw->scpw', tokens, kv_weight.reshape(model_width, blocks...  13.9 us
    all_gather x1, blocking collectives, finish(): lax.all_gather(contribution, 'sp')  13.2 us
    all_to_all x1, starting transfers between devices, local(): lax.all_to_all(projected.reshape(slot_count, pos_rows, block_width), 'sp'...  6.47 us
    reshape x1, local copies, waits for them, and re-layouts, local(): kv_weight.reshape(model_width, blocks, block_width)  6.43 us
    all_to_all x1, local copies, waits for them, and re-layouts, local(): lax.all_to_all(projected.reshape(slot_count, pos_rows, block_width), 'sp'...  6.18 us
  transfers between devices with their start and end apart: 1, of which 0 were waited for; matrix products, arithmetic and copies ran while one was open for 25% of the time, Pallas kernels for 0%

profile of v1, /device:TPU:0, one launch (start us, length us, event | category | flops | bytes accessed | tf_op | source)
XLA Modules:
  0.0 147.6 jit_solution(1743213823778053864)
XLA Ops:
  0.6 6.4 %copy.34 = bf16[2048,1024]{0,1:T(8,128)(2,1)} copy(bf16[2048,1024]{1,0:T(8,128)(2,1)} %param.7) | data formatting | bytes 8388608 | tf_op jit(solution)/shard_map/reshape | solution.py:45
  7.1 13.9 %fusion.2 = bf16[4,256,2048]{2,1,0:T(8,128)(2,1)} fusion(bf16[2048,4,256]{0,2,1:T(8,128)(2,1)} %bitcast.41, bf16[1,2048,2048]{2,1,0:T(8,128)(2,1)} %param.6), kind=kOutput, calls=%fused_computation.3 | convolution fusion | flops 8592031744 | bytes 16777216 | tf_op jit(solution)/shard_map/spd,dcw->scpw/dot_general | solution.py:42
  21.0 6.5 %all-to-all-start = ((bf16[4,2048,256]{1,2,0:T(8,128)(2,1)}), bf16[4,2048,256]{1,2,0:T(8,128)(2,1)}, u32[]{:S(2)}, u32[]{:S(2)}) async-start(bf16[4,2048,256]{1,2,0:T(8,128)(2,1)} %bitcast.38), calls=%async_computation | async-start | bytes 8388608 | tf_op jit(solution)/shard_map/all_to_all | solution.py:48
  27.5 0.1 reshape.120
  27.6 0.1 add.79
  27.7 2.8 %fusion.28 = (bf16[1,2,2048,256]{2,3,1,0:T(8,128)(2,1)S(1)}, bf16[1,2,2048,256]{2,3,1,0:T(8,128)(2,1)S(1)}) fusion(bf16[1,4,2048,256]{2,3,1,0:T(8,128)(2,1)} %bitcast.39), kind=kLoop, calls=%fused_computation.29 | loop fusion | bytes 8388608 | tf_op jit(solution)/shard_map/slice | solution.py:57
  30.4 0.7 fusion.24
  31.1 0.1 reshape.129
  31.2 29.8 %reduce-window.6 = f32[1,2,4,3,16,128]{5,4,3,2,1,0:T(8,128)S(1)} reduce-window(f32[1,2,4,3,16,128]{5,4,3,2,1,0:T(8,128)S(1)} %reshape.129, f32[]{:T(128)} %constant.56.clone.1), window={size=1x1x1x1x1x128 pad=0_0x0_0x0_0x0_0x0_0x0_127}, to_apply=%region_0.1 | reduce-window | flops 6242304 | bytes 393220 | tf_op jit(solution)/shard_map/reduce-window
  61.0 0.1 reshape.130
  61.1 0.2 copy.37
  61.3 1.5 %reduce-window.9 = f32[1,2,4,3,17]{4,3,2,1,0:T(4,128)S(1)} reduce-window(f32[1,2,4,3,16]{4,3,2,1,0:T(4,128)S(1)} %bitcast.47, f32[]{:T(128)} %constant.56.clone.1), window={size=1x1x1x1x16 pad=0_0x0_0x0_0x0_0x0_16}, to_apply=%region_1.2 | reduce-window | flops 6120 | bytes 3172 | tf_op jit(solution)/shard_map/reduce-window.1
  62.8 0.1 slice_bitcast_fusion
  62.9 0.1 broadcast.20
  63.0 0.1 reshape.125
  63.1 63.1 %all-gather = f32[8,4,3]{2,1,0:T(4,128)S(1)} all-gather(f32[2,4,3]{2,1,0:T(4,128)S(1)} %neg.35), channel_id=2, replica_groups=mesh['gr'=2,'sp'=4,'tp'=4] {'sp'}, dimensions={0}, use_global_device_ids=true | all-gather | bytes 480 | tf_op jit(solution)/shard_map/all_gather | solution.py:12
  126.2 0.1 copy.32
  126.3 0.2 while.16
  126.5 0.1 copy.33
  126.6 0.9 fusion.11
  127.6 0.1 all_gather_reshape.3
  127.7 13.2 %all_gather.8 = f32[4,1,1536]{2,1,0:T(1,128)S(1)} all-gather(f32[1,1,1536]{2,1,0:T(1,128)S(1)} %all_gather_reshape.3), channel_id=1, replica_groups=mesh['gr'=2,'sp'=4,'tp'=4] {'sp'}, dimensions={0}, use_global_device_ids=true | all-gather | bytes 30720 | tf_op jit(solution)/shard_map/all_gather | solution.py:29
  140.8 0.6 convert_element_type.28
  141.5 6.2 %copy.22 = bf16[4,2048,256]{2,1,0:T(8,128)(2,1)} copy(bf16[4,2048,256]{1,2,0:T(8,128)(2,1)} %all-to-all-done) | data formatting | bytes 8388608 | tf_op jit(solution)/shard_map/all_to_all | solution.py:48
  (14 shorter events, 0.2 us)
Async XLA Ops:
  21.0 6.5 %copy-start = (bf16[1,1536]{1,0:T(2,128)(2,1)S(1)}, bf16[1,1536]{1,0:T(2,128)(2,1)}, u32[]{:S(2)}) copy-start(bf16[1,1536]{1,0:T(2,128)(2,1)} %param.8) | copy-start | bytes 9220
  21.0 6.6 %copy-start.1 = (f32[24]{0:T(128)S(1)}, f32[24]{0:T(128)}, u32[]{:S(2)}) copy-start(f32[24]{0:T(128)} %param.9) | copy-start | bytes 292
  21.0 120.5 %all-to-all-start = ((bf16[4,2048,256]{1,2,0:T(8,128)(2,1)}), bf16[4,2048,256]{1,2,0:T(8,128)(2,1)}, u32[]{:S(2)}, u32[]{:S(2)}) async-start(bf16[4,2048,256]{1,2,0:T(8,128)(2,1)} %bitcast.38), calls=%async_computation | async-start | bytes 8388608 | tf_op jit(solution)/shard_map/all_to_all | solution.py:48
